TPU v7x, 32 devices: a whole 2x2x4 slice. The times are simulated.
32 devices in a mesh: sp: 16 (over z, y, core), tp: 2 (over x).
Axes of the slice: x: 2, y: 2, z: 4, core: 2. Of those that a mesh axis runs over, the one named last changes fastest.
Arguments:
- incoming_activity: bfloat16 [8192, 2048], P(('sp', 'tp')), may hold values from -6 to 6
- entry_standardize_factor: bfloat16 [2048], replicated, may hold values from 0.099609375 to 1.8984375
- recursive_entry_matrix: bfloat16 [2048, 2048], P(None, 'tp'), may hold values from -0.125 to 0.125
- final_switch_matrix: bfloat16 [2048, 2048], P(None, 'tp'), may hold values from -0.125 to 0.125
- averaging_entry_matrix: bfloat16 [2048, 1024], P(None, 'tp'), may hold values from -0.125 to 0.125
- percolumn_filter_coefficients: bfloat16 [4, 2048], P(None, 'tp'), may hold values from -3 to 3
- switch_tiled_matrices: bfloat16 [2, 2, 32, 64, 64], P(None, None, 'tp'), may hold values from -0.75 to 0.75
- prior_fading_odds: float32 [2, 2048], P(None, 'tp'), may hold values from 2.7 to 17
- speed_factors: float32 [2, 8192], P(None, 'sp'), may hold values from 0.4 to 2.5, as said below
- extra_fading_amounts: float32 [2, 8192], P(None, 'sp'), may hold values from -1.39 to 0, as said below
- averaging_cluster_matrices: bfloat16 [8, 128, 128], P('tp'), may hold values from -0.5 to 0.5
- averaging_feature_factor: bfloat16 [1024], P('tp'), may hold values from 0.099609375 to 1.8984375
- recursive_final_matrix: bfloat16 [2048, 2048], P('tp'), may hold values from -0.25 to 0.25
- averaging_final_matrix: bfloat16 [1024, 2048], P('tp'), may hold values from -0.1875 to 0.1875
Outputs:
- mixed: bfloat16 [8192, 2048], P(('sp', 'tp'))
Inputs may be any that keep to these rules, and one draw needn't show every extreme that they name: `speed_factors`: constant over each aligned block of 512 positions. `extra_fading_amounts`: each row has at most two nonzero entries.
All inputs are finite; a program needn't handle non-finite values.
Results may differ from a plain program's by a relative error of at most 0.017.
Values may be sent and summed in bfloat16 or wider, within the bound.
A program may use at most 128 MiB of HBM per device.

v0:
```python
import jax
import jax.numpy as jnp
from jax import lax
from jax.sharding import PartitionSpec as P

FADING_FACTOR = 8.0
epsilon = 1e-06
span_rows = 16


def padded(block, sides, width):
    for axis, dim in sides:
        count = lax.axis_size(axis)
        forward = [(i, i + 1) for i in range(count - 1)]
        backward = [(target, source) for source, target in forward]
        low = lax.ppermute(
            lax.slice_in_dim(block, block.shape[dim] - width, None, axis=dim), axis, forward
        )
        high = lax.ppermute(lax.slice_in_dim(block, 0, width, axis=dim), axis, backward)
        block = jnp.concatenate([low, block, high], axis=dim)
    return block


def combine(earlier, later):
    return (earlier[0] * later[0], later[0] * earlier[1] + later[1])


def product(left, right):
    return jnp.dot(left, right, preferred_element_type=jnp.float32)


def block_chain(log_keep, drive, backward):
    length, width = log_keep.shape
    count = length // span_rows
    logs = log_keep.reshape(count, span_rows, width)
    sources = drive.reshape(count, span_rows, width)
    running = jnp.cumsum(logs, axis=1)
    place = jnp.arange(span_rows, dtype=jnp.int32)
    if backward:
        running = running[:, -1:] - running + logs
        inside = place[None, :] >= place[:, None]
    else:
        inside = place[None, :] <= place[:, None]
    inside = inside[None, :, :, None]
    spread = running[:, :, None, :] - running[:, None, :, :]
    weights = jnp.where(inside, jnp.exp(jnp.where(inside, spread, 0.0)), 0.0)
    within = jnp.einsum("btsc,bsc->btc", weights, sources)
    decay = jnp.exp(running)
    ones = jnp.ones((1, width), jnp.float32)
    zeros = jnp.zeros((1, width), jnp.float32)
    if backward:
        ends = (decay[:, 0], within[:, 0])
        total_keep, total_state = lax.associative_scan(combine, ends, axis=0, reverse=True)
        prior_keep = jnp.concatenate([total_keep[1:], ones], axis=0)
        prior_state = jnp.concatenate([total_state[1:], zeros], axis=0)
    else:
        ends = (decay[:, -1], within[:, -1])
        total_keep, total_state = lax.associative_scan(combine, ends, axis=0)
        prior_keep = jnp.concatenate([ones, total_keep[:-1]], axis=0)
        prior_state = jnp.concatenate([zeros, total_state[:-1]], axis=0)
    keep_all = decay * prior_keep[:, None]
    local_all = within + decay * prior_state[:, None]
    return (keep_all.reshape(length, width), local_all.reshape(length, width))


def local(
    incoming_activity,
    entry_standardize_factor,
    recursive_entry_matrix,
    final_switch_matrix,
    averaging_entry_matrix,
    percolumn_filter_coefficients,
    switch_tiled_matrices,
    prior_fading_odds,
    speed_factors,
    extra_fading_amounts,
    averaging_cluster_matrices,
    averaging_feature_factor,
    recursive_final_matrix,
    averaging_final_matrix,
):
    state_width = recursive_entry_matrix.shape[1]
    pool_width = averaging_entry_matrix.shape[1]
    gain = entry_standardize_factor.astype(jnp.float32)
    values = lax.all_gather(incoming_activity, "tp", axis=0, tiled=True).astype(jnp.float32)
    scaled = values * lax.rsqrt(jnp.mean(values * values, axis=1, keepdims=True) + epsilon)
    normed = (scaled * gain).astype(jnp.bfloat16)
    projected = jnp.concatenate(
        [
            product(normed, weight).astype(jnp.bfloat16)
            for weight in (recursive_entry_matrix, final_switch_matrix, averaging_entry_matrix)
        ],
        axis=1,
    )
    length = projected.shape[0]
    state_input = projected[:, :state_width]
    gate_input = projected[:, state_width : 2 * state_width]
    pool_input = projected[:, 2 * state_width :]
    conv_rows = padded(state_input, (("sp", 0),), 2).astype(jnp.float32)
    filtered = percolumn_filter_coefficients[0].astype(jnp.float32) * conv_rows[0:length]
    for shift in range(1, percolumn_filter_coefficients.shape[0]):
        filtered = (
            filtered
            + percolumn_filter_coefficients[shift].astype(jnp.float32)
            * conv_rows[shift : shift + length]
        )
    filtered = filtered.astype(jnp.bfloat16)
    filtered_wide = filtered.astype(jnp.float32)
    blocks_here = switch_tiled_matrices.shape[2]
    block_width = switch_tiled_matrices.shape[3]
    gate_sums = jnp.einsum(
        "tbi,dqbij->tdqbj",
        filtered.reshape(length, blocks_here, block_width),
        switch_tiled_matrices,
        preferred_element_type=jnp.float32,
    ).reshape(length, 2, 2, state_width)
    remember_switch = jax.nn.sigmoid(gate_sums[:, :, 0])
    inlet = jax.nn.sigmoid(gate_sums[:, :, 1])
    fading_speed = jax.nn.softplus(-prior_fading_odds)
    logarithmic_persistence = (
        -FADING_FACTOR
        * jnp.transpose(speed_factors)[:, :, None]
        * remember_switch
        * fading_speed[None]
        + jnp.transpose(extra_fading_amounts)[:, :, None]
    )
    drive = jnp.sqrt(-jnp.expm1(2.0 * logarithmic_persistence)) * inlet * filtered_wide[:, None, :]
    forward_keep, forward_local = block_chain(logarithmic_persistence[:, 0], drive[:, 0], False)
    backward_keep, backward_local = block_chain(logarithmic_persistence[:, 1], drive[:, 1], True)
    zeros = jnp.zeros((state_width,), jnp.float32)
    summary = jnp.stack([forward_keep[-1], forward_local[-1], backward_keep[0], backward_local[0]])[
        None
    ]
    totals = lax.all_gather(summary, "sp", axis=0, tiled=True)
    place = lax.axis_index("sp")
    forward_all = lax.associative_scan(combine, (totals[:, 0], totals[:, 1]), axis=0)
    backward_all = lax.associative_scan(combine, (totals[:, 2], totals[:, 3]), axis=0, reverse=True)
    forward_before = jnp.concatenate([zeros[None], forward_all[1]], axis=0)
    backward_after = jnp.concatenate([backward_all[1], zeros[None]], axis=0)
    forward_carry = lax.dynamic_index_in_dim(forward_before, place, 0, keepdims=False)
    backward_carry = lax.dynamic_index_in_dim(backward_after, place + 1, 0, keepdims=False)
    state_sum = (
        forward_local
        + forward_keep * forward_carry[None]
        + backward_local
        + backward_keep * backward_carry[None]
    )
    state_mix = (jax.nn.gelu(gate_input.astype(jnp.float32)) * state_sum).astype(jnp.bfloat16)
    pool_rows = padded(pool_input, (("sp", 0),), 8).astype(jnp.float32)
    spans = []
    level = pool_rows
    for step in range(4):
        shift = 1 << step
        level = level[:-shift] + level[shift:]
        spans.append(level)
    group_width = averaging_cluster_matrices.shape[1]
    local_groups = pool_width // group_width
    group_index = (
        lax.axis_index("tp") * local_groups + jnp.arange(pool_width, dtype=jnp.int32) // group_width
    )
    window_code = group_index % 4
    position = lax.axis_index("sp") * length + jnp.arange(length, dtype=jnp.int32)
    total_length = length * lax.axis_size("sp")
    window_sum = jnp.zeros((length, pool_width), jnp.float32)
    counted = jnp.ones((length, pool_width), jnp.float32)
    for code in range(4):
        half = 1 << code
        begin = 8 - half
        chosen = (window_code == code)[None, :]
        window_count = (
            jnp.minimum(position + half, total_length) - jnp.maximum(position - half, 0)
        ).astype(jnp.float32)[:, None]
        window_sum = jnp.where(chosen, spans[code][begin : begin + length], window_sum)
        counted = jnp.where(chosen, window_count, counted)
    pooled = (window_sum / counted - pool_rows[8 : 8 + length]).astype(jnp.bfloat16)
    grouped = jnp.einsum(
        "tgi,gij->tgj",
        pooled.reshape(length, local_groups, group_width),
        averaging_cluster_matrices,
        preferred_element_type=jnp.float32,
    ).reshape(length, pool_width)
    pool_mix = (grouped * averaging_feature_factor.astype(jnp.float32)).astype(jnp.bfloat16)
    return lax.psum_scatter(
        (
            product(state_mix, recursive_final_matrix) + product(pool_mix, averaging_final_matrix)
        ).astype(jnp.bfloat16),
        "tp",
        scatter_dimension=0,
        tiled=True,
    )


def solution(mesh):
    in_specs = (
        P(("sp", "tp"), None),
        P(),
        P(None, "tp"),
        P(None, "tp"),
        P(None, "tp"),
        P(None, "tp"),
        P(None, None, "tp", None, None),
        P(None, "tp"),
        P(None, "sp"),
        P(None, "sp"),
        P("tp", None, None),
        P("tp"),
        P("tp", None),
        P("tp", None),
    )
    out_specs = P(("sp", "tp"), None)
    return jax.shard_map(local, mesh=mesh, in_specs=in_specs, out_specs=out_specs, check_vma=False)
```

profile of v0, /device:TPU:0, one launch (start us, length us, event | category | flops | bytes accessed | tf_op | source)
XLA Modules:
  0.0 250.9 jit_solution(8073936475268317214)
XLA Ops:
  10.5 34.2 %all-gather.4.cloned.1.call-done = bf16[512,2048]{1,0:T(8,128)(2,1)} async-done(((bf16[256,2048]{1,0:T(8,128)(2,1)}), bf16[512,2048]{1,0:T(8,128)(2,1)}) %all-gather.4.cloned.1.call-update) | async-done | bytes 2097168 | tf_op jit(solution)/shard_map/all_gather | solution.py:85
  47.0 4.7 %convolution_convert_fusion = bf16[512,1024]{1,0:T(8,128)(2,1)S(1)} fusion(bf16[2048,1024]{1,0:T(8,128)(2,1)} %param.16, bf16[512,2048]{1,0:T(8,128)(2,1)S(1)} %copy-done.9, f32[2048]{0:T(1024)S(1)} %convert_element_type.85, f32[512]{0:T(512)S(1)} %add_rsqrt_fusion), kind=kOutput, calls=%fused_computation.44 | convolution fusion | flops 2152202240 | bytes 7350272 | tf_op jit(solution)/shard_map/dot_general | solution.py:29
  56.0 4.4 %collective-permute-start.2 = (bf16[8,512]{1,0:T(8,128)(2,1)S(1)}, bf16[8,512]{1,0:T(8,128)(2,1)S(1)}, u32[]{:S(2)}, u32[]{:S(2)}) collective-permute-start(bf16[8,512]{1,0:T(8,128)(2,1)S(1)} %get-tuple-element.24), channel_id=1, source_target_pairs={{0,2},{2,4},{4,6},{6,8},{8,10},{10,12},{12,14},{14,16},{16,18},{18... | collective-permute-start | bytes 24584 | tf_op jit(solution)/shard_map/ppermute | solution.py:16
  62.1 2.6 %fusion.71 = (f32[512,1024]{1,0:T(8,128)}, bf16[512,1024]{1,0:T(8,128)(2,1)}) fusion(f32[516,1024]{1,0:T(8,128)S(1)} %maximum_convert_fusion, f32[1024]{0:T(1024)S(1)} %bitcast.154, f32[1024]{0:T(1024)S(1)} %bitcast.155, f32[1024]{0:T(1024)S(1)} %bitcast.153, f32[1024]{0:T(1024)S(1)} %bitcast.152), kind=kLoop, calls=%fused_computation.227 | loop fusion | flops 4718592 | bytes 11550720 | tf_op jit(solution)/shard_map/convert_element_type | solution.py:108
  67.1 2.5 fusion.96
  71.3 4.2 %fusion.74 = (f32[512,2,1,1024]{0,3,2,1:T(8,128)}, f32[512,2,1,1024]{0,3,2,1:T(8,128)}) fusion(f32[512,2,2,1024]{0,3,2,1:T(8,128)S(1)} %bitcast.122), kind=kLoop, calls=%fused_computation.229 | loop fusion | bytes 16777216 | tf_op jit(solution)/shard_map/slice | solution.py:117
  75.6 5.4 %copy.92 = f32[512,2,1,1024]{3,0,1,2:T(8,128)} copy(f32[512,2,1,1024]{0,3,2,1:T(8,128)} %get-tuple-element.12) | data formatting | bytes 8388608
  81.0 5.4 %copy.93 = f32[512,2,1,1024]{3,0,1,2:T(8,128)} copy(f32[512,2,1,1024]{0,3,2,1:T(8,128)} %get-tuple-element.13) | data formatting | bytes 8388608
  86.3 7.3 %fusion.3 = (f32[512,2,1024]{2,0,1:T(8,128)S(1)}, f32[512,2,1024]{2,0,1:T(8,128)S(1)}) fusion(f32[512,2,1,1024]{3,0,1,2:T(8,128)} %copy.93, f32[512,1024]{1,0:T(8,128)} %get-tuple-element.7, f32[512,2]{0,1:T(2,128)S(1)} %bitcast.158, f32[2,1024]{1,0:T(2,128)S(1)} %compare_select_fusion, f32[512,2,1,1024]{3,0,1,2:T(8,128)} %copy.92, ...), kind=kLoop, calls=%fused_computation.8 | loop fusion | flops 13631488 | bytes 18890752 | tf_op jit(solution)/shard_map/mul | solution.py:127
  93.6 3.3 %fusion.75 = (f32[512,1,1024]{2,0,1:T(8,128)}, f32[512,1,1024]{2,0,1:T(8,128)S(1)}, f32[512,1,1024]{2,0,1:T(8,128)}, f32[512,1,1024]{2,0,1:T(8,128)}) fusion(f32[512,2,1024]{2,0,1:T(8,128)S(1)} %get-tuple-element.6, f32[512,2,1024]{2,0,1:T(8,128)S(1)} %get-tuple-element.5), kind=kLoop, calls=%fused_computation.230 | loop fusion | bytes 16777216 | tf_op jit(solution)/shard_map/slice | solution.py:128
  98.9 3.6 %fusion.73 = (f32[32,16,1024]{2,0,1:T(8,128)S(1)}, f32[32,16,1024]{2,0,1:T(8,128)}, f32[32,16,1024]{2,0,1:T(8,128)}) fusion(f32[32,16,1024]{2,1,0:T(8,128)S(1)} %bitcast.124, f32[32,16,1024]{2,0,1:T(8,128)S(1)} %fusion.20, f32[32,1024]{1,0:T(8,128)S(1)} %slice_bitcast_fusion.2), kind=kLoop, calls=%fused_computation.228 | loop fusion | flops 1048576 | bytes 10616832 | tf_op jit(solution)/shard_map/exp | solution.py:48
  102.5 3.0 %copy.66 = f32[32,16,1024]{2,1,0:T(8,128)S(1)} copy(f32[32,16,1024]{2,0,1:T(8,128)} %get-tuple-element.10) | data formatting | bytes 4194304 | tf_op jit(solution)/shard_map/add | solution.py:40
  105.5 12.3 %multiply_reduce_fusion = f32[32,1024,16]{1,2,0:T(8,128)S(1)} fusion(f32[32,1024,16]{1,2,0:T(8,128)S(1)} %bitcast.139, f32[32,16,1024]{2,1,0:T(8,128)S(1)} %copy.66, pred[16,16]{1,0:T(8,128)(4,1)S(1)} %iota_compare_fusion), kind=kLoop, calls=%fused_computation | loop fusion | flops 41418752 | bytes 6291712
  120.6 4.3 %fusion.95 = (f32[32,16,1024]{2,0,1:T(8,128)S(1)}, f32[32,16,1024]{2,0,1:T(8,128)}) fusion(f32[32,16,1024]{2,1,0:T(8,128)} %bitcast.125), kind=kOutput, calls=%fused_computation.250 | output fusion | flops 7864320 | bytes 6291456 | tf_op jit(solution)/shard_map/jit(cumsum)/reduce_window_sum | solution.py:37
  125.0 3.0 %copy.59 = f32[32,16,1024]{2,1,0:T(8,128)S(1)} copy(f32[32,16,1024]{2,0,1:T(8,128)} %get-tuple-element.97) | data formatting | bytes 4194304 | tf_op jit(solution)/shard_map/jit(cumsum)/reduce_window_sum | solution.py:37
  128.0 12.1 %multiply_reduce_fusion.1 = f32[32,1024,16]{1,2,0:T(8,128)S(1)} fusion(f32[32,1024,16]{1,2,0:T(8,128)S(1)} %bitcast.138, f32[32,16,1024]{2,1,0:T(8,128)S(1)} %copy.59, pred[16,16]{1,0:T(8,128)(4,1)S(1)} %iota_compare_fusion.1), kind=kLoop, calls=%fused_computation.1 | loop fusion | flops 41418752 | bytes 6291712
  142.2 4.1 %copy.64 = f32[32,16,1024]{2,1,0:T(8,128)} copy(f32[32,16,1024]{2,0,1:T(8,128)} %get-tuple-element.11) | data formatting | bytes 4194304 | tf_op jit(solution)/shard_map/sub | solution.py:40
  148.1 3.7 %multiply_add_fusion = f32[32,16,1024]{2,0,1:T(8,128)S(1)} fusion(f32[32,1024]{1,0:T(8,128)S(1)} %concatenate.110, f32[32,1024,16]{1,2,0:T(8,128)} %copy-done.3, f32[32,16,1024]{2,0,1:T(8,128)} %get-tuple-element.10), kind=kLoop, calls=%fused_computation.39 | loop fusion | flops 1048576 | bytes 6422528 | tf_op jit(solution)/shard_map/add | solution.py:62
  154.8 2.8 %bitcast_multiply_fusion.2 = f32[512,1024]{1,0:T(8,128)S(1)} fusion(f32[32,16,1024]{2,1,0:T(8,128)} %copy.64, f32[32,1024]{1,0:T(8,128)S(1)} %concatenate.105, f32[512,2,1024]{2,0,1:T(8,128)} %copy-done.1), kind=kLoop, calls=%fused_computation.32 | loop fusion | flops 1048576 | bytes 6422528 | tf_op jit(solution)/shard_map/mul | solution.py:61
  159.8 3.7 %broadcast_multiply_fusion = (f32[32,16,1024]{2,0,1:T(8,128)S(1)}, f32[32,16,1024]{2,0,1:T(8,128)S(1)}) fusion(f32[32,1024]{1,0:T(8,128)S(1)} %concatenate.100, f32[32,16,1024]{2,0,1:T(8,128)} %get-tuple-element.97, f32[32,1024]{1,0:T(8,128)S(1)} %concatenate.95, f32[32,1024,16]{1,2,0:T(8,128)} %copy-done.4), kind=kLoop, calls=%fused_computation.62 | loop fusion | flops 1572864 | bytes 8650752 | tf_op jit(solution)/shard_map/mul | solution.py:61
  167.5 24.6 %all-gather.1 = f32[16,4,1024]{2,1,0:T(4,128)S(1)} all-gather(f32[1,4,1024]{2,1,0:T(4,128)S(1)} %maximum_bitcast_fusion), channel_id=2, replica_groups=mesh['sp'=16,'tp'=2] {'sp'}, dimensions={0}, use_global_device_ids=true | all-gather | bytes 278528 | tf_op jit(solution)/shard_map/all_gather | solution.py:134
  195.4 13.8 %fusion.28 = f32[512,2048]{1,0:T(8,128)} fusion(bf16[1024,2048]{1,0:T(8,128)(2,1)} %param.26, f32[512,1024]{1,0:T(8,128)} %copy-done.5, f32[512,1024]{1,0:T(8,128)} %bitcast.133, f32[512,1024]{1,0:T(8,128)} %bitcast.137, f32[512,1024]{1,0:T(8,128)} %bitcast.135, bf16[2048,1024]{1,0:T(8,128)(2,1)} %param.17, f32[1024]{0:T(1024)S(1)} %bitcast.157, ...), kind=kOutput, calls=%fused_computation.63 | convolution fusion | flops 4308074496 | bytes 23087104 | tf_op jit(solution)/shard_map/dot_general | solution.py:29
  212.9 2.6 %add_convert_fusion = bf16[512,2048]{1,0:T(8,128)(2,1)} fusion(f32[512,2048]{1,0:T(8,128)S(1)} %copy-done.2, bf16[512,512]{0,1:T(8,128)(2,1)S(1)} %fusion.27, bf16[512,2048]{1,0:T(8,128)(2,1)S(1)} %copy-done), kind=kOutput, calls=%fused_computation.12 | convolution fusion | flops 1075838976 | bytes 8912896 | tf_op jit(solution)/shard_map/dot_general | solution.py:29
  215.6 28.4 %reduce-scatter.2.cloned.1.call-done = bf16[256,2048]{1,0:T(8,128)(2,1)} async-done(((bf16[512,2048]{1,0:T(8,128)(2,1)}), bf16[256,2048]{1,0:T(8,128)(2,1)}) %reduce-scatter.2.cloned.1.call-update) | async-done | bytes 1048592 | tf_op jit(solution)/shard_map/reduce_scatter | solution.py:183
  (337 shorter events, 39.6 us)
Async XLA Ops:
  6.5 205.6 %copy-start = (bf16[512,2048]{1,0:T(8,128)(2,1)S(1)}, bf16[512,2048]{1,0:T(8,128)(2,1)}, u32[]{:S(2)}) copy-start(bf16[512,2048]{1,0:T(8,128)(2,1)} %param.27) | copy-start | bytes 6291460
  6.5 3.9 %copy-start.16 = (f32[2,512]{1,0:T(2,128)S(1)}, f32[2,512]{1,0:T(2,128)}, u32[]{:S(2)}) copy-start(f32[2,512]{1,0:T(2,128)} %param.22) | copy-start | bytes 12292
  6.5 3.9 %copy-start.15 = (f32[2,1024]{1,0:T(2,128)S(1)}, f32[2,1024]{1,0:T(2,128)}, u32[]{:S(2)}) copy-start(f32[2,1024]{1,0:T(2,128)} %param.21) | copy-start | bytes 24580
  6.5 3.9 %copy-start.14 = (bf16[4,1024]{1,0:T(4,128)(2,1)S(1)}, bf16[4,1024]{1,0:T(4,128)(2,1)}, u32[]{:S(2)}) copy-start(bf16[4,1024]{1,0:T(4,128)(2,1)} %param.19) | copy-start | bytes 24580
  6.5 38.2 %all-gather.4.cloned.1.call-start = ((), (), s32[]{:S(2)}) async-start(), calls=%async_computation.1 | async-start | bytes 3145728 | tf_op jit(solution)/shard_map/all_gather | solution.py:85
  7.3 236.6 %reduce-scatter.2.cloned.1.call-start = ((), (), s32[]{:S(2)}) async-start(), calls=%async_computation.2 | async-start | bytes 3145728 | tf_op jit(solution)/shard_map/reduce_scatter | solution.py:183
  44.7 2.2 copy-start.9
  47.0 7.7 %copy-start.18 = (bf16[2048,512]{1,0:T(8,128)(2,1)S(1)}, bf16[2048,512]{1,0:T(8,128)(2,1)}, u32[]{:S(2)}) copy-start(bf16[2048,512]{1,0:T(8,128)(2,1)} %param.18) | copy-start | bytes 6291460
  51.8 10.0 %collective-permute-start = (bf16[2,1024]{1,0:T(2,128)(2,1)S(1)}, bf16[2,1024]{1,0:T(2,128)(2,1)S(1)}, u32[]{:S(2)}, u32[]{:S(2)}) collective-permute-start(bf16[2,1024]{1,0:T(2,128)(2,1)S(1)} %get-tuple-element.22), channel_id=1, source_target_pairs={{0,2},{2,4},{4,6},{6,8},{8,10},{10,12},{12,14},{14,16},{16,18},{18... | collective-permute-start | bytes 12296 | tf_op jit(solution)/shard_map/ppermute | solution.py:16
  53.3 8.4 %collective-permute-start.1 = (bf16[2,1024]{1,0:T(2,128)(2,1)S(1)}, bf16[2,1024]{1,0:T(2,128)(2,1)S(1)}, u32[]{:S(2)}, u32[]{:S(2)}) collective-permute-start(bf16[2,1024]{1,0:T(2,128)(2,1)S(1)} %get-tuple-element.23), channel_id=1, source_target_pairs={{2,0},{4,2},{6,4},{8,6},{10,8},{12,10},{14,12},{16,14},{18,16},{20... | collective-permute-start | bytes 12296 | tf_op jit(solution)/shard_map/ppermute | solution.py:19
  56.0 6.1 %copy-start.12 = (bf16[512,512]{1,0:T(8,128)(2,1)}, bf16[512,512]{1,0:T(8,128)(2,1)S(1)}, u32[]{:S(2)}) copy-start(bf16[512,512]{1,0:T(8,128)(2,1)S(1)} %convolution_convert_fusion.2) | copy-start | bytes 1572868
  56.0 153.2 %collective-permute-start.2 = (bf16[8,512]{1,0:T(8,128)(2,1)S(1)}, bf16[8,512]{1,0:T(8,128)(2,1)S(1)}, u32[]{:S(2)}, u32[]{:S(2)}) collective-permute-start(bf16[8,512]{1,0:T(8,128)(2,1)S(1)} %get-tuple-element.24), channel_id=1, source_target_pairs={{0,2},{2,4},{4,6},{6,8},{8,10},{10,12},{12,14},{14,16},{16,18},{18... | collective-permute-start | bytes 24584 | tf_op jit(solution)/shard_map/ppermute | solution.py:16
  60.4 148.8 %collective-permute-start.3 = (bf16[8,512]{1,0:T(8,128)(2,1)S(1)}, bf16[8,512]{1,0:T(8,128)(2,1)S(1)}, u32[]{:S(2)}, u32[]{:S(2)}) collective-permute-start(bf16[8,512]{1,0:T(8,128)(2,1)S(1)} %get-tuple-element.25), channel_id=1, source_target_pairs={{2,0},{4,2},{6,4},{8,6},{10,8},{12,10},{14,12},{16,14},{18,16},{20... | collective-permute-start | bytes 24584 | tf_op jit(solution)/shard_map/ppermute | solution.py:19
  81.0 5.4 %copy-start.17 = (f32[2,512]{1,0:T(2,128)S(1)}, f32[2,512]{1,0:T(2,128)}, u32[]{:S(2)}) copy-start(f32[2,512]{1,0:T(2,128)} %param.23) | copy-start | bytes 12292
  93.6 3.9 %copy-start.1 = (f32[512,2,1024]{2,0,1:T(8,128)}, f32[512,2,1024]{2,0,1:T(8,128)S(1)}, u32[]{:S(2)}) copy-start(f32[512,2,1024]{2,0,1:T(8,128)S(1)} %get-tuple-element.6) | copy-start | bytes 12582916
  102.5 3.0 %copy-start.11 = (f32[512,1,1024]{2,0,1:T(8,128)S(1)}, f32[512,1,1024]{2,0,1:T(8,128)}, u32[]{:S(2)}) copy-start(f32[512,1,1024]{2,0,1:T(8,128)} %get-tuple-element.98) | copy-start | bytes 6291460
  125.0 3.0 %copy-start.10 = (f32[512,1,1024]{2,0,1:T(8,128)S(1)}, f32[512,1,1024]{2,0,1:T(8,128)}, u32[]{:S(2)}) copy-start(f32[512,1,1024]{2,0,1:T(8,128)} %get-tuple-element.99) | copy-start | bytes 6291460
  140.1 1.3 copy-start.4
  153.1 1.4 copy-start.6
  157.5 1.4 copy-start.5
  164.7 1.3 copy-start.7
  166.1 1.4 copy-start.8
  195.4 13.8 %copy-start.13 = (bf16[512,512]{1,0:T(8,128)(2,1)S(1)}, bf16[512,512]{1,0:T(8,128)(2,1)}, u32[]{:S(2)}) copy-start(bf16[512,512]{1,0:T(8,128)(2,1)} %copy-done.12) | copy-start | bytes 1572868
  210.7 2.2 copy-start.2
  (2 other events, 2.2 us)
Sparse Core Ops, SparseCore 0:
  8.9 35.8 all-gather.3
  215.7 28.1 reduce-scatter.1
where the time goes:
time: 256 us; the launch traced here: 251 us
  waiting for transfers between devices  63.3 us (25%)
  other arithmetic  59.6 us (23%)
  local copies, waits for them, and re-layouts  53.3 us (21%)
  matrix products  26.1 us (10%)
  blocking collectives  24.6 us (10%)
  between operations  15.4 us (6%)
  starting transfers between devices  8.68 us (3%)
    all_gather x1, waiting for transfers between devices, local(): lax.all_gather(incoming_activity, 'tp', axis=0, tiled=True)  34.2 us
    reduce_scatter x1, waiting for transfers between devices, local(): lax.psum_scatter((product(state_mix, recursive_final_matrix) + product(po...  28.4 us
    all_gather x1, blocking collectives, local(): totals = lax.all_gather(summary, 'sp', axis=0, tiled=True)  24.6 us
    unnamed x3, other arithmetic  24.5 us
    dot_general x4, matrix products, product(): return jnp.dot(left, right, preferred_element_type=jnp.float32)  22.4 us
    unnamed x51, local copies, waits for them, and re-layouts  18.9 us
    mul x1, other arithmetic, local(): jnp.sqrt(-jnp.expm1(2.0 * logarithmic_persistence)) * inlet  7.26 us
    mul x2, other arithmetic, block_chain(): keep_all = decay * prior_keep[:, None]  6.51 us
  transfers between devices with their start and end apart: 6, of which 2 were waited for; matrix products, arithmetic and copies ran while one was open for 48% of the time, Pallas kernels for 0%

commit v1 on v0

v1 whole, which is shorter than its diff:
```python
import functools

import jax
import jax.numpy as jnp
from jax import lax
from jax.experimental import pallas as pl
from jax.experimental.pallas import tpu as pltpu
from jax.sharding import PartitionSpec as P

FADING_FACTOR = 8.0
epsilon = 1e-06
EDGE = 16
MESH = pl.DeviceIdType.MESH
F32 = jnp.float32
BF16 = jnp.bfloat16


def product(left, right):
    return jnp.dot(left, right, preferred_element_type=F32)


def sigmoid(x):
    return 1.0 / (1.0 + jnp.exp(-x))


def small_softplus(odds):
    e = jnp.exp(-odds)
    z = e / (2.0 + e)
    y = z * z
    return 2.0 * z * (1.0 + y * (1.0 / 3.0 + y * (1.0 / 5.0 + y * (1.0 / 7.0))))


def one_less_exp(y, exp_y):
    near = 1.0 + y * (1.0 / 6.0) * (1.0 + y * (1.0 / 7.0))
    near = 1.0 + y * (1.0 / 5.0) * near
    near = 1.0 + y * (1.0 / 4.0) * near
    near = 1.0 + y * (1.0 / 3.0) * near
    near = 1.0 + y * (1.0 / 2.0) * near
    return jnp.where(y > -0.25, -y * near, 1.0 - exp_y)


def kernel(
    n_sp,
    n_tp,
    x_hbm,
    gain_ref,
    ws_hbm,
    wg_hbm,
    wp_hbm,
    conv_ref,
    switch_ref,
    odds_ref,
    cols_ref,
    cluster_ref,
    factor_ref,
    wso_hbm,
    wpo_hbm,
    out_ref,
    x_own,
    x_far,
    halo,
    normed,
    ws,
    wg,
    wp,
    wso,
    wpo,
    s_buf,
    g_buf,
    p_buf,
    filt,
    diag,
    sums,
    keep,
    loc,
    summary,
    totals,
    mix,
    pool_mix,
    part,
    landed,
    w_sem,
    ag_send,
    ag_recv,
    halo_send,
    halo_recv,
    c_send,
    c_recv,
    rs_send,
    rs_recv,
):
    sp = lax.axis_index("sp")
    tp = lax.axis_index("tp")
    rows, depth = x_own.shape
    length = rows * n_tp
    width = ws.shape[1]
    pool_width = wp.shape[1]

    gathers = []
    nxt = lax.rem(sp + 1, n_sp)
    prv = lax.rem(sp + n_sp - 1, n_sp)

    def halo_copy(side, tp_to, slot):
        src = x_hbm.at[pl.ds(rows - EDGE if side == 0 else 0, EDGE)]
        return pltpu.make_async_remote_copy(
            src_ref=src,
            dst_ref=halo.at[side],
            send_sem=halo_send.at[side, slot],
            recv_sem=halo_recv.at[side],
            device_id=(nxt if side == 0 else prv, tp_to),
            device_id_type=MESH,
        )

    for side, sender in ((0, n_tp - 1), (1, 0)):

        @pl.when(tp == sender)
        def _():
            for j in range(n_tp):
                halo_copy(side, j, j).start()

    for k in range(1, n_tp):
        copy = pltpu.make_async_remote_copy(
            src_ref=x_hbm,
            dst_ref=x_far.at[pl.ds((k - 1) * rows, rows)],
            send_sem=ag_send.at[k],
            recv_sem=ag_recv.at[k],
            device_id=(sp, lax.rem(tp + k, n_tp)),
            device_id_type=MESH,
        )
        copy.start()
        gathers.append(copy)
    loads = []
    for i, (src, dst) in enumerate(
        (
            (x_hbm, x_own),
            (ws_hbm, ws),
            (wg_hbm, wg),
            (wp_hbm, wp),
            (wso_hbm, wso),
            (wpo_hbm, wpo),
        )
    ):
        copy = pltpu.make_async_copy(src, dst, w_sem.at[i])
        copy.start()
        loads.append(copy)

    gain = gain_ref[...].astype(F32)

    def normalise(src, count, at):
        @pl.loop(0, count // 16)
        def _(i):
            at_row = pl.multiple_of(i * 16, 16)
            values = src[pl.ds(at_row, 16), :].astype(F32)
            mean = jnp.mean(values * values, axis=1, keepdims=True)
            scaled = values * lax.rsqrt(mean + epsilon)
            normed[pl.ds(pl.multiple_of(at + at_row, 16), 16), :] = (scaled * gain).astype(BF16)

    tile = min(256, width)
    ptile = min(256, pool_width)

    def owner_row(k):
        return pl.multiple_of(EDGE + lax.rem(tp + n_tp - k, n_tp) * rows, 16)

    def project(weights, buf, step, first, count, pieces, act):
        @pl.loop(0, weights.shape[1] // step)
        def _(c):
            at = pl.ds(pl.multiple_of(c * step, step), step)
            value = product(normed[pl.ds(first, count), :], weights[:, at]).astype(BF16)
            value = act(value.astype(F32))
            for begin, size, row in pieces:
                buf[pl.ds(row, size), at] = value[begin : begin + size]

    same = lambda v: v
    gelu = functools.partial(jax.nn.gelu, approximate=True)

    half = switch_ref.shape[2]
    spread = (
        lax.broadcasted_iota(jnp.int32, (half, tile), 1) % half
        == lax.broadcasted_iota(jnp.int32, (half, tile), 0)
    ).astype(F32).astype(BF16)
    on_diag = (
        lax.broadcasted_iota(jnp.int32, (tile, tile), 0) // half
        == lax.broadcasted_iota(jnp.int32, (tile, tile), 1) // half
    )
    for m in range(4):

        @pl.loop(0, width // tile)
        def _(g):
            at = pl.ds(pl.multiple_of(g * tile, tile), tile)
            wide = product(switch_ref[m, at, :], spread)
            diag[m, at, :] = jnp.where(on_diag, wide, 0.0).astype(BF16)

    loads[0].wait()
    normalise(x_own, rows, 0)
    own = ((0, rows, owner_row(0)),)
    loads[1].wait()
    project(ws, s_buf, tile, 0, rows, own, same)
    loads[2].wait()
    project(wg, g_buf, tile, 0, rows, own, gelu)
    loads[3].wait()
    project(wp, p_buf, ptile, 0, rows, own, same)

    far = rows * (n_tp - 1)
    for side in range(2):
        halo_copy(side, 0, 0).wait_recv()
    normalise(halo.at[0], EDGE, rows + far)
    normalise(halo.at[1], EDGE, rows + far + EDGE)

    @pl.when(sp == 0)
    def _():
        normed[pl.ds(rows + far, EDGE), :] = jnp.zeros((EDGE, depth), BF16)

    @pl.when(sp == n_sp - 1)
    def _():
        normed[pl.ds(rows + far + EDGE, EDGE), :] = jnp.zeros((EDGE, depth), BF16)

    for copy in gathers:
        copy.wait_recv()
    normalise(x_far, far, rows)
    pieces = [((k - 1) * rows, rows, owner_row(k)) for k in range(1, n_tp)]
    edges = [(far, EDGE, 0), (far + EDGE, EDGE, EDGE + length)]
    project(ws, s_buf, tile, rows, far + 2 * EDGE, pieces + edges, same)

    total_rows = length + 2 * EDGE

    @pl.loop(0, width // tile)
    def _(g):
        at = pl.ds(pl.multiple_of(g * tile, tile), tile)
        taps = conv_ref[:, at].astype(F32)
        x = s_buf[:, at]
        y = taps[0:1] * pltpu.roll(x, 2, 0)
        y = y + taps[1:2] * pltpu.roll(x, 1, 0)
        y = y + taps[2:3] * x
        y = y + taps[3:4] * pltpu.roll(x, total_rows - 1, 0)
        y = y[EDGE : EDGE + length].astype(BF16)
        filt[:, at] = y.astype(F32)
        for m in range(4):
            sums[m, :, at] = product(y, diag[m, at, :])

    lanes = min(512, width)
    groups = length // 8
    place = lax.broadcasted_iota(jnp.int32, (8, lanes), 0)

    for lane in range(0, width, lanes):
        at = pl.ds(lane, lanes)
        rates = -FADING_FACTOR * small_softplus(odds_ref[:, at])

        def step(i, carry):
            result = []
            for d in range(2):
                group = i if d == 0 else groups - 1 - i
                here = pl.ds(pl.multiple_of(group * 8, 8), 8)
                cols = cols_ref[here, :]
                log_keep = cols[:, d : d + 1] * sigmoid(sums[2 * d, here, at]) * rates[d : d + 1]
                log_keep = log_keep + cols[:, 2 + d : 3 + d]
                a = jnp.exp(log_keep)
                root = jnp.sqrt(one_less_exp(2.0 * log_keep, a * a))
                b = root * sigmoid(sums[2 * d + 1, here, at]) * filt[here, at]
                for k in (1, 2, 4):
                    if d == 0:
                        inside, shift = place >= k, k
                    else:
                        inside, shift = place < 8 - k, 8 - k
                    b = jnp.where(inside, b + a * pltpu.roll(b, shift, 0), b)
                    a = jnp.where(inside, a * pltpu.roll(a, shift, 0), a)
                kept, state = carry[2 * d], carry[2 * d + 1]
                b = b + a * state
                a = a * kept
                keep[d, here, at] = a
                loc[d, here, at] = b
                last = 7 if d == 0 else 0
                result += [a[last : last + 1], b[last : last + 1]]
            return tuple(result)

        one, zero = jnp.ones((1, lanes), F32), jnp.zeros((1, lanes), F32)
        ends = lax.fori_loop(0, groups, step, (one, zero, one, zero), unroll=2)
        for d in range(2):
            summary[d, 0:1, at] = ends[2 * d]
            summary[d, 1:2, at] = ends[2 * d + 1]

    carries = []
    for k in range(1, n_sp):
        to = lax.rem(sp + k, n_sp)
        way = jnp.where(to > sp, 0, 1)
        copy = pltpu.make_async_remote_copy(
            src_ref=summary.at[way],
            dst_ref=totals.at[k],
            send_sem=c_send.at[k],
            recv_sem=c_recv.at[k],
            device_id=(to, tp),
            device_id_type=MESH,
        )
        copy.start()
        carries.append(copy)

    project(wg, g_buf, tile, rows, far, pieces, gelu)
    project(wp, p_buf, ptile, rows, far + 2 * EDGE, pieces + edges, same)
    gw = cluster_ref.shape[1]
    local_groups = pool_width // gw
    position = sp * length + lax.broadcasted_iota(jnp.int32, (length, gw), 0)
    total_length = length * n_sp
    for j in range(local_groups):
        x = p_buf[:, j * gw : (j + 1) * gw]
        level = x
        code_here = lax.rem(tp * local_groups + j, 4)
        codes = (j % 4,) if local_groups % 4 == 0 else range(4)
        pooled = None
        for code in range(codes[-1] + 1):
            h = 1 << code
            level = level + pltpu.roll(level, total_rows - h, 0)
            if code not in codes:
                continue
            window = pltpu.roll(level, h, 0)[EDGE : EDGE + length]
            counted = jnp.minimum(position + h, total_length) - jnp.maximum(position - h, 0)
            value = window / counted.astype(F32)
            pooled = value if pooled is None else jnp.where(code_here == code, value, pooled)
        pooled = (pooled - x[EDGE : EDGE + length]).astype(BF16)
        mapped = product(pooled, cluster_ref[j]) * factor_ref[:, j * gw : (j + 1) * gw].astype(F32)
        pool_mix[:, j * gw : (j + 1) * gw] = mapped.astype(BF16)

    for copy in carries:
        copy.wait_recv()
    forward = jnp.zeros((1, width), F32)
    backward = jnp.zeros((1, width), F32)
    for k in range(n_sp - 1, 0, -1):
        valid = k <= sp
        forward = jnp.where(valid, totals[k, 0:1, :] * forward + totals[k, 1:2, :], forward)
    for k in range(1, n_sp):
        valid = k > sp
        backward = jnp.where(valid, totals[k, 0:1, :] * backward + totals[k, 1:2, :], backward)

    loads[4].wait()
    loads[5].wait()
    columns = wso.shape[1]
    parts = part.shape[1]
    ctile = columns // parts

    def mix_rows(first):
        @pl.loop(0, rows // 16)
        def _(i):
            here = pl.ds(pl.multiple_of(first + i * 16, 16), 16)
            state = loc[0, here, :] + keep[0, here, :] * forward
            state = state + loc[1, here, :] + keep[1, here, :] * backward
            gate = g_buf[pl.ds(pl.multiple_of(EDGE + first + i * 16, 16), 16), :]
            mix[here, :] = (gate * state).astype(BF16)

    def share(first, c):
        here = pl.ds(first, rows)
        at = pl.ds(c * ctile, ctile)
        return product(mix[here, :], wso[:, at]) + product(pool_mix[here, :], wpo[:, at])

    scatters = []
    for k in range(1, n_tp):
        to = lax.rem(tp + k, n_tp)
        first = pl.multiple_of(to * rows, 16)
        mix_rows(first)
        for c in range(parts):
            part[k - 1, c] = share(first, c).astype(BF16)
            scatters.append(
                pltpu.make_async_remote_copy(
                    src_ref=part.at[k - 1, c],
                    dst_ref=landed.at[k - 1, c],
                    send_sem=rs_send.at[k - 1, c],
                    recv_sem=rs_recv.at[k - 1, c],
                    device_id=(sp, to),
                    device_id_type=MESH,
                )
            )
            if len(scatters) > 1:
                scatters[-2].start()
    first = pl.multiple_of(tp * rows, 16)
    mix_rows(first)
    if scatters:
        scatters[-1].start()
    for c in range(parts):
        x_total = share(first, c)
        for k in range(1, n_tp):
            scatters[(k - 1) * parts + c].wait_recv()
            x_total = x_total + landed[k - 1, c].astype(F32)
        out_ref[:, c * ctile : (c + 1) * ctile] = x_total.astype(BF16)

    for copy in gathers + carries + scatters:
        copy.wait_send()
    for side, sender in ((0, n_tp - 1), (1, 0)):

        @pl.when(tp == sender)
        def _():
            for j in range(n_tp):
                halo_copy(side, j, j).wait_send()


def local(
    n_sp,
    n_tp,
    incoming_activity,
    entry_standardize_factor,
    recursive_entry_matrix,
    final_switch_matrix,
    averaging_entry_matrix,
    percolumn_filter_coefficients,
    switch_tiled_matrices,
    prior_fading_odds,
    speed_factors,
    extra_fading_amounts,
    averaging_cluster_matrices,
    averaging_feature_factor,
    recursive_final_matrix,
    averaging_final_matrix,
):
    rows, depth = incoming_activity.shape
    length = rows * n_tp
    width = recursive_entry_matrix.shape[1]
    pool_width = averaging_entry_matrix.shape[1]
    columns = recursive_final_matrix.shape[1]
    half = switch_tiled_matrices.shape[-1]
    cols = jnp.transpose(jnp.concatenate([speed_factors, extra_fading_amounts], axis=0))
    parts = 4
    tile = min(256, width)
    hbm = pl.BlockSpec(memory_space=pl.ANY)
    vmem = pl.BlockSpec(memory_space=pltpu.VMEM)
    dma = pltpu.SemaphoreType.DMA
    peers = max(n_tp - 1, 1)
    padded = length + 2 * EDGE
    return pl.pallas_call(
        functools.partial(kernel, n_sp, n_tp),
        out_shape=jax.ShapeDtypeStruct((rows, columns), BF16),
        in_specs=[hbm, vmem, hbm, hbm, hbm, vmem, vmem, vmem, vmem, vmem, vmem, hbm, hbm],
        out_specs=vmem,
        scratch_shapes=[
            pltpu.VMEM((rows, depth), BF16),
            pltpu.VMEM((rows * peers, depth), BF16),
            pltpu.VMEM((2, EDGE, depth), BF16),
            pltpu.VMEM((padded, depth), BF16),
            pltpu.VMEM((depth, width), BF16),
            pltpu.VMEM((depth, width), BF16),
            pltpu.VMEM((depth, pool_width), BF16),
            pltpu.VMEM((width, columns), BF16),
            pltpu.VMEM((pool_width, columns), BF16),
            pltpu.VMEM((padded, width), F32),
            pltpu.VMEM((padded, width), F32),
            pltpu.VMEM((padded, pool_width), F32),
            pltpu.VMEM((length, width), F32),
            pltpu.VMEM((4, width, tile), BF16),
            pltpu.VMEM((4, length, width), F32),
            pltpu.VMEM((2, length, width), F32),
            pltpu.VMEM((2, length, width), F32),
            pltpu.VMEM((2, 2, width), F32),
            pltpu.VMEM((n_sp, 2, width), F32),
            pltpu.VMEM((length, width), BF16),
            pltpu.VMEM((length, pool_width), BF16),
            pltpu.VMEM((peers, parts, rows, columns // parts), BF16),
            pltpu.VMEM((peers, parts, rows, columns // parts), BF16),
            dma((6,)),
            dma((n_tp,)),
            dma((n_tp,)),
            dma((2, n_tp)),
            dma((2,)),
            dma((n_sp,)),
            dma((n_sp,)),
            dma((peers, parts)),
            dma((peers, parts)),
        ],
        compiler_params=pltpu.CompilerParams(
            has_side_effects=True, vmem_limit_bytes=63 * 1024 * 1024
        ),
    )(
        incoming_activity,
        entry_standardize_factor.reshape(1, depth),
        recursive_entry_matrix,
        final_switch_matrix,
        averaging_entry_matrix,
        percolumn_filter_coefficients,
        switch_tiled_matrices.reshape(4, width, half),
        prior_fading_odds,
        cols,
        averaging_cluster_matrices,
        averaging_feature_factor.reshape(1, pool_width),
        recursive_final_matrix,
        averaging_final_matrix,
    )


def solution(mesh):
    in_specs = (
        P(("sp", "tp"), None),
        P(),
        P(None, "tp"),
        P(None, "tp"),
        P(None, "tp"),
        P(None, "tp"),
        P(None, None, "tp", None, None),
        P(None, "tp"),
        P(None, "sp"),
        P(None, "sp"),
        P("tp", None, None),
        P("tp"),
        P("tp", None),
        P("tp", None),
    )
    out_specs = P(("sp", "tp"), None)
    body = functools.partial(local, mesh.shape["sp"], mesh.shape["tp"])
    return jax.shard_map(body, mesh=mesh, in_specs=in_specs, out_specs=out_specs, check_vma=False)
```

time: 256 us -> 95.1 us (0.37); the launches traced: 251 us -> 94.9 us
  Pallas kernels: 0 us -> 88.4 us
  waiting for transfers between devices: 63.3 us -> 0 us
  other arithmetic: 59.6 us -> 0.71 us
  local copies, waits for them, and re-layouts: 53.3 us -> 5.72 us
  matrix products: 26.1 us -> 0 us
  blocking collectives: 24.6 us -> 0 us
  between operations: 15.4 us -> 0.01 us
  starting transfers between devices: 8.68 us -> 0 us
    pallas_call x0 -> x1, Pallas kernels: none -> 88.4 us  [local(): pl.pallas_call(functools.partial(kernel, n_sp, n_tp), out_shape=jax.Shape...]
    all_gather x1 -> x0, waiting for transfers between devices: 34.2 us -> none  [local(): lax.all_gather(incoming_activity, 'tp', axis=0, tiled=True)]
    reduce_scatter x1 -> x0, waiting for transfers between devices: 28.4 us -> none  [local(): lax.psum_scatter((product(state_mix, recursive_final_matrix) + product(po...]
    all_gather x1 -> x0, blocking collectives: 24.6 us -> none  [local(): totals = lax.all_gather(summary, 'sp', axis=0, tiled=True)]
    unnamed x3 -> x0, other arithmetic: 24.5 us -> none
    dot_general x5 -> x0, matrix products: 23.7 us -> none  [the longest x4 22.4 us: product(): return jnp.dot(left, right, preferred_element_type=jnp.float32)]
    unnamed x51 -> x1, local copies, waits for them, and re-layouts: 18.9 us -> 2.3 us
    mul x17 -> x0, other arithmetic: 14 us -> none  [the longest x1 7.26 us: local(): jnp.sqrt(-jnp.expm1(2.0 * logarithmic_persistence)) * inlet]
  transfers between devices with their start and end apart: 6 -> 0, of which waited for: 2 -> 0; matrix products, arithmetic and copies ran while one was open for 48% -> 0% of each run, Pallas kernels for 0% -> 0%
where the time goes in v1:
time: 95.1 us; the launch traced here: 94.9 us
  Pallas kernels  88.4 us (93%)
  local copies, waits for them, and re-layouts  5.72 us (6%)
    pallas_call x1, Pallas kernels, local(): pl.pallas_call(functools.partial(kernel, n_sp, n_tp), out_shape=jax.Shape...  88.4 us
    unnamed x1, local copies, waits for them, and re-layouts  2.3 us

profile of v1, /device:TPU:0, one launch (start us, length us, event | category | flops | bytes accessed | tf_op | source)
XLA Modules:
  0.0 94.9 jit_solution(1038492185326531955)
XLA Ops:
  0.0 1.3 %reshape.11.factor_ref = bf16[1,512]{1,0:T(2,128)(2,1)} reshape(bf16[512]{0:T(512)(128)(2,1)} %param.25) | data formatting | bytes 2048 | tf_op jit(solution)/shard_map/reshape | solution.py:477
  1.3 1.3 %reshape.9.gain_ref = bf16[1,2048]{1,0:T(2,128)(2,1)} reshape(bf16[2048]{0:T(1024)(128)(2,1)} %param.15) | data formatting | bytes 8192 | tf_op jit(solution)/shard_map/reshape | solution.py:468
  2.6 0.7 pad_maximum_fusion
  3.3 0.9 copy.17
  4.1 88.4 %shard_map.136 = bf16[256,2048]{1,0:T(8,128)(2,1)} custom-call(bf16[256,2048]{1,0:T(8,128)(2,1)} %x_hbm.1, bf16[1,2048]{1,0:T(2,128)(2,1)} %reshape.9.gain_ref, bf16[2048,1024]{1,0:T(8,128)(2,1)} %ws_hbm.1, bf16[2048,1024]{1,0:T(8,128)(2,1)} %wg_hbm.1, bf16[2048,512]{1,0:T(8,128)(2,1)} %wp_hbm.1, bf16[4,1024]{1,0:T(4,128)(2,1)} %conv_ref.1, ...), custom_call_target="tpu_custom_call" | custom-call | tf_op jit(solution)/shard_map/pallas_call | solution.py:424
  92.6 2.3 %copy.19 = bf16[256,2048]{1,0:T(8,128)(2,1)} copy(bf16[256,2048]{1,0:T(8,128)(2,1)} %shard_map.136) | data formatting | bytes 2097152

commit v2 on v1

--- a/solution.py
+++ b/solution.py
@@ -19,10 +19,6 @@
     return jnp.dot(left, right, preferred_element_type=F32)
 
 
-def sigmoid(x):
-    return 1.0 / (1.0 + jnp.exp(-x))
-
-
 def small_softplus(odds):
     e = jnp.exp(-odds)
     z = e / (2.0 + e)
@@ -30,13 +26,9 @@
     return 2.0 * z * (1.0 + y * (1.0 / 3.0 + y * (1.0 / 5.0 + y * (1.0 / 7.0))))
 
 
-def one_less_exp(y, exp_y):
-    near = 1.0 + y * (1.0 / 6.0) * (1.0 + y * (1.0 / 7.0))
-    near = 1.0 + y * (1.0 / 5.0) * near
-    near = 1.0 + y * (1.0 / 4.0) * near
-    near = 1.0 + y * (1.0 / 3.0) * near
-    near = 1.0 + y * (1.0 / 2.0) * near
-    return jnp.where(y > -0.25, -y * near, 1.0 - exp_y)
+def minus_tanh(u):
+    near = -u * (1.0 - u * u * (1.0 / 3.0))
+    return jnp.where(u > -0.015625, near, jnp.tanh(-u))
 
 
 def kernel(
@@ -50,7 +42,8 @@
     conv_ref,
     switch_ref,
     odds_ref,
-    cols_ref,
+    speed_ref,
+    extra_ref,
     cluster_ref,
     factor_ref,
     wso_hbm,
@@ -59,6 +52,8 @@
     x_own,
     x_far,
     halo,
+    near,
+    cols,
     normed,
     ws,
     wg,
@@ -73,6 +68,8 @@
     sums,
     keep,
     loc,
+    ends_buf,
+    carry_in,
     summary,
     totals,
     mix,
@@ -84,6 +81,8 @@
     ag_recv,
     halo_send,
     halo_recv,
+    near_send,
+    near_recv,
     c_send,
     c_recv,
     rs_send,
@@ -118,17 +117,36 @@
             for j in range(n_tp):
                 halo_copy(side, j, j).start()
 
-    for k in range(1, n_tp):
+    up_tp = lax.rem(tp + 1, n_tp)
+    down_tp = lax.rem(tp + n_tp - 1, n_tp)
+    up = (jnp.where(tp == n_tp - 1, nxt, sp), up_tp)
+    down = (jnp.where(tp == 0, prv, sp), down_tp)
+    nears = []
+    for side, to in ((0, up), (1, down)):
         copy = pltpu.make_async_remote_copy(
-            src_ref=x_hbm,
-            dst_ref=x_far.at[pl.ds((k - 1) * rows, rows)],
-            send_sem=ag_send.at[k],
-            recv_sem=ag_recv.at[k],
-            device_id=(sp, lax.rem(tp + k, n_tp)),
+            src_ref=x_hbm.at[pl.ds(rows - EDGE if side == 0 else 0, EDGE)],
+            dst_ref=near.at[side],
+            send_sem=near_send.at[side],
+            recv_sem=near_recv.at[side],
+            device_id=to,
             device_id_type=MESH,
         )
         copy.start()
-        gathers.append(copy)
+        nears.append(copy)
+    pieces_in = ag_send.shape[1]
+    piece = rows // pieces_in
+    for k in range(1, n_tp):
+        for q in range(pieces_in):
+            copy = pltpu.make_async_remote_copy(
+                src_ref=x_hbm.at[pl.ds(q * piece, piece)],
+                dst_ref=x_far.at[pl.ds((k - 1) * rows + q * piece, piece)],
+                send_sem=ag_send.at[k, q],
+                recv_sem=ag_recv.at[k, q],
+                device_id=(sp, lax.rem(tp + k, n_tp)),
+                device_id_type=MESH,
+            )
+            copy.start()
+            gathers.append(copy)
     loads = []
     for i, (src, dst) in enumerate(
         (
@@ -144,13 +162,15 @@
         copy.start()
         loads.append(copy)
 
-    gain = gain_ref[...].astype(F32)
-
-    def normalise(src, count, at):
+    gain = gain_ref[...].astype(F32).reshape(1, depth)
+    fill = jnp.zeros((6, length), F32)
+    cols[...] = jnp.transpose(jnp.concatenate([extra_ref[...], fill], axis=0))
+
+    def normalise(src, count, at, begin=0):
         @pl.loop(0, count // 16)
         def _(i):
             at_row = pl.multiple_of(i * 16, 16)
-            values = src[pl.ds(at_row, 16), :].astype(F32)
+            values = src[pl.ds(pl.multiple_of(begin + at_row, 16), 16), :].astype(F32)
             mean = jnp.mean(values * values, axis=1, keepdims=True)
             scaled = values * lax.rsqrt(mean + epsilon)
             normed[pl.ds(pl.multiple_of(at + at_row, 16), 16), :] = (scaled * gain).astype(BF16)
@@ -188,95 +208,129 @@
         def _(g):
             at = pl.ds(pl.multiple_of(g * tile, tile), tile)
             wide = product(switch_ref[m, at, :], spread)
-            diag[m, at, :] = jnp.where(on_diag, wide, 0.0).astype(BF16)
-
+            diag[m, at, :] = jnp.where(on_diag, 0.5 * wide, 0.0).astype(BF16)
+
+    lanes = min(512, width)
+    groups = rows // 8
+    place = lax.broadcasted_iota(jnp.int32, (8, lanes), 0)
+    window = rows + 2 * EDGE
+
+    def chunk(owner):
+        base = pl.multiple_of(owner * rows, 16)
+
+        @pl.loop(0, width // tile)
+        def _(g):
+            at = pl.ds(pl.multiple_of(g * tile, tile), tile)
+            taps = conv_ref[:, at].astype(F32)
+            x = s_buf[pl.ds(base, window), at]
+            y = taps[0:1] * pltpu.roll(x, 2, 0)
+            y = y + taps[1:2] * pltpu.roll(x, 1, 0)
+            y = y + taps[2:3] * x
+            y = y + taps[3:4] * pltpu.roll(x, window - 1, 0)
+            y = y[EDGE : EDGE + rows].astype(BF16)
+            filt[:, at] = 0.5 * y.astype(F32)
+            for m in range(4):
+                sums[m, :, at] = product(y, diag[m, at, :])
+
+        for lane in range(0, width, lanes):
+            at = pl.ds(lane, lanes)
+            rates = -0.5 * FADING_FACTOR * small_softplus(odds_ref[:, at]) * speed_ref[:, 0:1]
+
+            def step(i, carry):
+                result = []
+                for d in range(2):
+                    group = i if d == 0 else groups - 1 - i
+                    here = pl.ds(pl.multiple_of(group * 8, 8), 8)
+                    there = pl.ds(pl.multiple_of(base + group * 8, 8), 8)
+                    rate = rates[d : d + 1]
+                    log_keep = jnp.tanh(sums[2 * d, here, at]) * rate + rate
+                    log_keep = log_keep + cols[there, d : d + 1]
+                    a = jnp.exp(log_keep)
+                    square = minus_tanh(log_keep) * (1.0 + a * a)
+                    root = square * lax.rsqrt(square + 1e-37)
+                    f = filt[here, at]
+                    b = root * (f + f * jnp.tanh(sums[2 * d + 1, here, at]))
+                    for k in (1, 2, 4):
+                        if d == 0:
+                            inside, shift = place >= k, k
+                        else:
+                            inside, shift = place < 8 - k, 8 - k
+                        b = jnp.where(inside, b + a * pltpu.roll(b, shift, 0), b)
+                        a = jnp.where(inside, a * pltpu.roll(a, shift, 0), a)
+                    kept, state = carry[2 * d], carry[2 * d + 1]
+                    b = b + a * state
+                    a = a * kept
+                    keep[d, there, at] = a
+                    loc[d, there, at] = b
+                    last = 7 if d == 0 else 0
+                    result += [a[last : last + 1], b[last : last + 1]]
+                return tuple(result)
+
+            one, zero = jnp.ones((1, lanes), F32), jnp.zeros((1, lanes), F32)
+            ends = lax.fori_loop(0, groups, step, (one, zero, one, zero), unroll=2)
+            for m in range(4):
+                ends_buf[owner, m : m + 1, at] = ends[m]
+
+    far = rows * (n_tp - 1)
+    total_rows = length + 2 * EDGE
+    edge_at = rows + far
     loads[0].wait()
     normalise(x_own, rows, 0)
+    for copy in nears:
+        copy.wait_recv()
+    for side in range(2):
+        normalise(near.at[side], EDGE, rows + side * EDGE)
+
+    @pl.when(jnp.logical_and(sp == 0, tp == 0))
+    def _():
+        normed[pl.ds(rows, EDGE), :] = jnp.zeros((EDGE, depth), BF16)
+
+    @pl.when(jnp.logical_and(sp == n_sp - 1, tp == n_tp - 1))
+    def _():
+        normed[pl.ds(rows + EDGE, EDGE), :] = jnp.zeros((EDGE, depth), BF16)
+
     own = ((0, rows, owner_row(0)),)
+    own_edges = (
+        (rows, EDGE, pl.multiple_of(tp * rows, 16)),
+        (rows + EDGE, EDGE, pl.multiple_of(EDGE + tp * rows + rows, 16)),
+    )
     loads[1].wait()
-    project(ws, s_buf, tile, 0, rows, own, same)
+    project(ws, s_buf, tile, 0, rows + 2 * EDGE, own + own_edges, same)
+    chunk(tp)
     loads[2].wait()
     project(wg, g_buf, tile, 0, rows, own, gelu)
     loads[3].wait()
     project(wp, p_buf, ptile, 0, rows, own, same)
 
-    far = rows * (n_tp - 1)
     for side in range(2):
         halo_copy(side, 0, 0).wait_recv()
-    normalise(halo.at[0], EDGE, rows + far)
-    normalise(halo.at[1], EDGE, rows + far + EDGE)
+        normalise(halo.at[side], EDGE, edge_at + side * EDGE)
 
     @pl.when(sp == 0)
     def _():
-        normed[pl.ds(rows + far, EDGE), :] = jnp.zeros((EDGE, depth), BF16)
+        normed[pl.ds(edge_at, EDGE), :] = jnp.zeros((EDGE, depth), BF16)
 
     @pl.when(sp == n_sp - 1)
     def _():
-        normed[pl.ds(rows + far + EDGE, EDGE), :] = jnp.zeros((EDGE, depth), BF16)
-
-    for copy in gathers:
+        normed[pl.ds(edge_at + EDGE, EDGE), :] = jnp.zeros((EDGE, depth), BF16)
+
+    for n, copy in enumerate(gathers):
         copy.wait_recv()
-    normalise(x_far, far, rows)
+        normalise(x_far, piece, rows + n * piece, n * piece)
     pieces = [((k - 1) * rows, rows, owner_row(k)) for k in range(1, n_tp)]
     edges = [(far, EDGE, 0), (far + EDGE, EDGE, EDGE + length)]
     project(ws, s_buf, tile, rows, far + 2 * EDGE, pieces + edges, same)
-
-    total_rows = length + 2 * EDGE
-
-    @pl.loop(0, width // tile)
-    def _(g):
-        at = pl.ds(pl.multiple_of(g * tile, tile), tile)
-        taps = conv_ref[:, at].astype(F32)
-        x = s_buf[:, at]
-        y = taps[0:1] * pltpu.roll(x, 2, 0)
-        y = y + taps[1:2] * pltpu.roll(x, 1, 0)
-        y = y + taps[2:3] * x
-        y = y + taps[3:4] * pltpu.roll(x, total_rows - 1, 0)
-        y = y[EDGE : EDGE + length].astype(BF16)
-        filt[:, at] = y.astype(F32)
-        for m in range(4):
-            sums[m, :, at] = product(y, diag[m, at, :])
-
-    lanes = min(512, width)
-    groups = length // 8
-    place = lax.broadcasted_iota(jnp.int32, (8, lanes), 0)
-
-    for lane in range(0, width, lanes):
-        at = pl.ds(lane, lanes)
-        rates = -FADING_FACTOR * small_softplus(odds_ref[:, at])
-
-        def step(i, carry):
-            result = []
-            for d in range(2):
-                group = i if d == 0 else groups - 1 - i
-                here = pl.ds(pl.multiple_of(group * 8, 8), 8)
-                cols = cols_ref[here, :]
-                log_keep = cols[:, d : d + 1] * sigmoid(sums[2 * d, here, at]) * rates[d : d + 1]
-                log_keep = log_keep + cols[:, 2 + d : 3 + d]
-                a = jnp.exp(log_keep)
-                root = jnp.sqrt(one_less_exp(2.0 * log_keep, a * a))
-                b = root * sigmoid(sums[2 * d + 1, here, at]) * filt[here, at]
-                for k in (1, 2, 4):
-                    if d == 0:
-                        inside, shift = place >= k, k
-                    else:
-                        inside, shift = place < 8 - k, 8 - k
-                    b = jnp.where(inside, b + a * pltpu.roll(b, shift, 0), b)
-                    a = jnp.where(inside, a * pltpu.roll(a, shift, 0), a)
-                kept, state = carry[2 * d], carry[2 * d + 1]
-                b = b + a * state
-                a = a * kept
-                keep[d, here, at] = a
-                loc[d, here, at] = b
-                last = 7 if d == 0 else 0
-                result += [a[last : last + 1], b[last : last + 1]]
-            return tuple(result)
-
-        one, zero = jnp.ones((1, lanes), F32), jnp.zeros((1, lanes), F32)
-        ends = lax.fori_loop(0, groups, step, (one, zero, one, zero), unroll=2)
-        for d in range(2):
-            summary[d, 0:1, at] = ends[2 * d]
-            summary[d, 1:2, at] = ends[2 * d + 1]
+    for k in range(1, n_tp):
+        chunk(lax.rem(tp + n_tp - k, n_tp))
+
+    for d in range(2):
+        kept, state = jnp.ones((1, width), F32), jnp.zeros((1, width), F32)
+        for j in range(n_tp) if d == 0 else range(n_tp - 1, -1, -1):
+            step_keep = ends_buf[j, 2 * d : 2 * d + 1, :]
+            state = step_keep * state + ends_buf[j, 2 * d + 1 : 2 * d + 2, :]
+            kept = step_keep * kept
+        summary[d, 0:1, :] = kept
+        summary[d, 1:2, :] = state
 
     carries = []
     for k in range(1, n_sp):
@@ -297,6 +351,7 @@
     project(wp, p_buf, ptile, rows, far + 2 * EDGE, pieces + edges, same)
     gw = cluster_ref.shape[1]
     local_groups = pool_width // gw
+    factors = factor_ref[...].astype(F32).reshape(1, pool_width)
     position = sp * length + lax.broadcasted_iota(jnp.int32, (length, gw), 0)
     total_length = length * n_sp
     for j in range(local_groups):
@@ -310,12 +365,12 @@
             level = level + pltpu.roll(level, total_rows - h, 0)
             if code not in codes:
                 continue
-            window = pltpu.roll(level, h, 0)[EDGE : EDGE + length]
+            spanned = pltpu.roll(level, h, 0)[EDGE : EDGE + length]
             counted = jnp.minimum(position + h, total_length) - jnp.maximum(position - h, 0)
-            value = window / counted.astype(F32)
+            value = spanned / counted.astype(F32)
             pooled = value if pooled is None else jnp.where(code_here == code, value, pooled)
         pooled = (pooled - x[EDGE : EDGE + length]).astype(BF16)
-        mapped = product(pooled, cluster_ref[j]) * factor_ref[:, j * gw : (j + 1) * gw].astype(F32)
+        mapped = product(pooled, cluster_ref[j]) * factors[:, j * gw : (j + 1) * gw]
         pool_mix[:, j * gw : (j + 1) * gw] = mapped.astype(BF16)
 
     for copy in carries:
@@ -329,13 +384,24 @@
         valid = k > sp
         backward = jnp.where(valid, totals[k, 0:1, :] * backward + totals[k, 1:2, :], backward)
 
+    for j in range(n_tp):
+        carry_in[j, 0:1, :] = forward
+        forward = ends_buf[j, 0:1, :] * forward + ends_buf[j, 1:2, :]
+    for j in range(n_tp - 1, -1, -1):
+        carry_in[j, 1:2, :] = backward
+        backward = ends_buf[j, 2:3, :] * backward + ends_buf[j, 3:4, :]
+
     loads[4].wait()
     loads[5].wait()
     columns = wso.shape[1]
     parts = part.shape[1]
     ctile = columns // parts
 
-    def mix_rows(first):
+    def mix_rows(owner):
+        first = owner * rows
+        forward = carry_in[owner, 0:1, :]
+        backward = carry_in[owner, 1:2, :]
+
         @pl.loop(0, rows // 16)
         def _(i):
             here = pl.ds(pl.multiple_of(first + i * 16, 16), 16)
@@ -353,7 +419,7 @@
     for k in range(1, n_tp):
         to = lax.rem(tp + k, n_tp)
         first = pl.multiple_of(to * rows, 16)
-        mix_rows(first)
+        mix_rows(to)
         for c in range(parts):
             part[k - 1, c] = share(first, c).astype(BF16)
             scatters.append(
@@ -369,7 +435,7 @@
             if len(scatters) > 1:
                 scatters[-2].start()
     first = pl.multiple_of(tp * rows, 16)
-    mix_rows(first)
+    mix_rows(tp)
     if scatters:
         scatters[-1].start()
     for c in range(parts):
@@ -379,7 +445,7 @@
             x_total = x_total + landed[k - 1, c].astype(F32)
         out_ref[:, c * ctile : (c + 1) * ctile] = x_total.astype(BF16)
 
-    for copy in gathers + carries + scatters:
+    for copy in gathers + nears + carries + scatters:
         copy.wait_send()
     for side, sender in ((0, n_tp - 1), (1, 0)):
 
@@ -413,7 +479,6 @@
     pool_width = averaging_entry_matrix.shape[1]
     columns = recursive_final_matrix.shape[1]
     half = switch_tiled_matrices.shape[-1]
-    cols = jnp.transpose(jnp.concatenate([speed_factors, extra_fading_amounts], axis=0))
     parts = 4
     tile = min(256, width)
     hbm = pl.BlockSpec(memory_space=pl.ANY)
@@ -424,12 +489,14 @@
     return pl.pallas_call(
         functools.partial(kernel, n_sp, n_tp),
         out_shape=jax.ShapeDtypeStruct((rows, columns), BF16),
-        in_specs=[hbm, vmem, hbm, hbm, hbm, vmem, vmem, vmem, vmem, vmem, vmem, hbm, hbm],
+        in_specs=[hbm, vmem, hbm, hbm, hbm, vmem, vmem, vmem, vmem, vmem, vmem, vmem, hbm, hbm],
         out_specs=vmem,
         scratch_shapes=[
             pltpu.VMEM((rows, depth), BF16),
             pltpu.VMEM((rows * peers, depth), BF16),
             pltpu.VMEM((2, EDGE, depth), BF16),
+            pltpu.VMEM((2, EDGE, depth), BF16),
+            pltpu.VMEM((length, 8), F32),
             pltpu.VMEM((padded, depth), BF16),
             pltpu.VMEM((depth, width), BF16),
             pltpu.VMEM((depth, width), BF16),
@@ -439,11 +506,13 @@
             pltpu.VMEM((padded, width), F32),
             pltpu.VMEM((padded, width), F32),
             pltpu.VMEM((padded, pool_width), F32),
-            pltpu.VMEM((length, width), F32),
+            pltpu.VMEM((rows, width), F32),
             pltpu.VMEM((4, width, tile), BF16),
-            pltpu.VMEM((4, length, width), F32),
+            pltpu.VMEM((4, rows, width), F32),
             pltpu.VMEM((2, length, width), F32),
             pltpu.VMEM((2, length, width), F32),
+            pltpu.VMEM((n_tp, 4, width), F32),
+            pltpu.VMEM((n_tp, 2, width), F32),
             pltpu.VMEM((2, 2, width), F32),
             pltpu.VMEM((n_sp, 2, width), F32),
             pltpu.VMEM((length, width), BF16),
@@ -451,9 +520,11 @@
             pltpu.VMEM((peers, parts, rows, columns // parts), BF16),
             pltpu.VMEM((peers, parts, rows, columns // parts), BF16),
             dma((6,)),
-            dma((n_tp,)),
-            dma((n_tp,)),
+            dma((n_tp, 4)),
+            dma((n_tp, 4)),
             dma((2, n_tp)),
+            dma((2,)),
+            dma((2,)),
             dma((2,)),
             dma((n_sp,)),
             dma((n_sp,)),
@@ -465,16 +536,17 @@
         ),
     )(
         incoming_activity,
-        entry_standardize_factor.reshape(1, depth),
+        entry_standardize_factor,
         recursive_entry_matrix,
         final_switch_matrix,
         averaging_entry_matrix,
         percolumn_filter_coefficients,
         switch_tiled_matrices.reshape(4, width, half),
         prior_fading_odds,
-        cols,
+        speed_factors,
+        extra_fading_amounts,
         averaging_cluster_matrices,
-        averaging_feature_factor.reshape(1, pool_width),
+        averaging_feature_factor,
         recursive_final_matrix,
         averaging_final_matrix,
     )

time: 95.1 us -> 83.2 us (0.87)
  Pallas kernels: 88.4 us -> 80.7 us
  local copies, waits for them, and re-layouts: 5.72 us -> 2.3 us
    pallas_call x1, Pallas kernels: 88.4 us -> 80.7 us  [local(): pl.pallas_call(functools.partial(kernel, n_sp, n_tp), out_shape=jax.Shape...]
    reshape x2 -> x0, local copies, waits for them, and re-layouts: 2.55 us -> none  [the longest x1 1.28 us: local(): entry_standardize_factor.reshape(1, depth)]
where the time goes in v2:
time: 83.2 us; the launch traced here: 83 us
  Pallas kernels  80.7 us (97%)
  local copies, waits for them, and re-layouts  2.3 us (3%)
    pallas_call x1, Pallas kernels, local(): pl.pallas_call(functools.partial(kernel, n_sp, n_tp), out_shape=jax.Shape...  80.7 us
    unnamed x1, local copies, waits for them, and re-layouts  2.3 us

profile of v2, /device:TPU:0, one launch (start us, length us, event | category | flops | bytes accessed | tf_op | source)
XLA Modules:
  0.0 83.0 jit_solution(2810598284601134992)
XLA Ops:
  0.0 80.7 %shard_map.136 = bf16[256,2048]{1,0:T(8,128)(2,1)} custom-call(bf16[256,2048]{1,0:T(8,128)(2,1)} %x_hbm.1, bf16[2048]{0:T(1024)(128)(2,1)} %gain_ref.1, bf16[2048,1024]{1,0:T(8,128)(2,1)} %ws_hbm.1, bf16[2048,1024]{1,0:T(8,128)(2,1)} %wg_hbm.1, bf16[2048,512]{1,0:T(8,128)(2,1)} %wp_hbm.1, bf16[4,1024]{1,0:T(4,128)(2,1)} %conv_ref.1, ...), custom_call_target="tpu_custom_call" | custom-call | tf_op jit(solution)/shard_map/pallas_call | solution.py:489
  80.7 2.3 %copy.16 = bf16[256,2048]{1,0:T(8,128)(2,1)} copy(bf16[256,2048]{1,0:T(8,128)(2,1)} %shard_map.136) | data formatting | bytes 2097152

commit v3 on v2

--- a/solution.py
+++ b/solution.py
@@ -267,7 +267,7 @@
                 return tuple(result)
 
             one, zero = jnp.ones((1, lanes), F32), jnp.zeros((1, lanes), F32)
-            ends = lax.fori_loop(0, groups, step, (one, zero, one, zero), unroll=2)
+            ends = lax.fori_loop(0, groups, step, (one, zero, one, zero), unroll=4)
             for m in range(4):
                 ends_buf[owner, m : m + 1, at] = ends[m]
 

time: 83.2 us -> 82.2 us (0.988)
  Pallas kernels: 80.7 us -> 79.7 us
    pallas_call x1, Pallas kernels: 80.7 us -> 79.7 us  [local(): pl.pallas_call(functools.partial(kernel, n_sp, n_tp), out_shape=jax.Shape...]
where the time goes in v3:
time: 82.2 us; the launch traced here: 82 us
  Pallas kernels  79.7 us (97%)
  local copies, waits for them, and re-layouts  2.3 us (3%)
    pallas_call x1, Pallas kernels, local(): pl.pallas_call(functools.partial(kernel, n_sp, n_tp), out_shape=jax.Shape...  79.7 us
    unnamed x1, local copies, waits for them, and re-layouts  2.3 us

profile of v3, /device:TPU:0, one launch (start us, length us, event | category | flops | bytes accessed | tf_op | source)
XLA Modules:
  0.0 82.0 jit_solution(4886608143917031516)
XLA Ops:
  0.0 79.7 %shard_map.136 = bf16[256,2048]{1,0:T(8,128)(2,1)} custom-call(bf16[256,2048]{1,0:T(8,128)(2,1)} %x_hbm.1, bf16[2048]{0:T(1024)(128)(2,1)} %gain_ref.1, bf16[2048,1024]{1,0:T(8,128)(2,1)} %ws_hbm.1, bf16[2048,1024]{1,0:T(8,128)(2,1)} %wg_hbm.1, bf16[2048,512]{1,0:T(8,128)(2,1)} %wp_hbm.1, bf16[4,1024]{1,0:T(4,128)(2,1)} %conv_ref.1, ...), custom_call_target="tpu_custom_call" | custom-call | tf_op jit(solution)/shard_map/pallas_call | solution.py:489
  79.7 2.3 %copy.16 = bf16[256,2048]{1,0:T(8,128)(2,1)} copy(bf16[256,2048]{1,0:T(8,128)(2,1)} %shard_map.136) | data formatting | bytes 2097152
